TPU v7x, 32 devices: a whole 2x2x4 slice. The times are simulated.
32 devices in a mesh: sp: 8 (over z, x), tp: 4 (over y, core).
Axes of the slice: x: 2, y: 2, z: 4, core: 2. Of those that a mesh axis runs over, the one named last changes fastest.
Arguments:
- out_grad: bfloat16 [1024, 2048], P('sp', 'tp'), may hold values from -6 to 6
- moe_input: bfloat16 [1024, 2048], P('sp', 'tp'), may hold values from -6 to 6
- route_weight: float32 [1024, 2], P('sp'), may hold values from 0.2 to 1
- route_ids: int32 [1024, 2], P('sp'), may hold values from 0 to 7, all different within a row; in each aligned block of 128 rows (0 to 127, 128 to 255, ...) at most 64 rows name the same one
- gate_proj: bfloat16 [8, 2048, 2816], P('sp', None, 'tp'), may hold values from -0.125 to 0.125
- up_proj: bfloat16 [8, 2048, 2816], P('sp', None, 'tp'), may hold values from -0.125 to 0.125
- down_proj: bfloat16 [8, 2816, 2048], P('sp', 'tp'), may hold values from -0.109375 to 0.109375
- out_proj: bfloat16 [2048, 2048], P(None, 'tp'), may hold values from -0.125 to 0.125
- conv_out: bfloat16 [1024, 2048], P('sp', 'tp'), may hold values from -6 to 6
- gate_b: bfloat16 [1024, 2048], P('sp', 'tp'), may hold values from -6 to 6
- gate_c: bfloat16 [1024, 2048], P('sp', 'tp'), may hold values from -6 to 6
- value_v: bfloat16 [1024, 2048], P('sp', 'tp'), may hold values from -6 to 6
- conv_taps: float32 [3, 2048], P(None, 'tp'), may hold values from -3 to 3
Outputs:
- grad_gate: bfloat16 [8, 2048, 2816], P('sp', None, 'tp')
- grad_up: bfloat16 [8, 2048, 2816], P('sp', None, 'tp')
- grad_down: bfloat16 [8, 2816, 2048], P('sp', 'tp')
- grad_out: float32 [2048, 2048], P('sp', 'tp')
- grad_b: bfloat16 [1024, 2048], P('sp', 'tp')
- grad_c: bfloat16 [1024, 2048], P('sp', 'tp')
- grad_v: bfloat16 [1024, 2048], P('sp', 'tp')
Inputs may be any that keep to these rules, and one draw needn't show every extreme that they name: `route_ids`: each row names two different experts; within the 128 rows of one index of sp no expert is named by more than 64 rows, a bound that some block reaches.
All inputs are finite; a program needn't handle non-finite values.
Results may differ from a plain program's by a relative error of at most 0.019.
Values may be sent and summed in bfloat16 or wider, within the bound.
A program may use at most 64 MiB of HBM per device.

v0:
```python
import functools

import jax
import jax.numpy as jnp
from jax import lax
from jax.experimental import pallas as pl
from jax.experimental.pallas import tpu as pltpu
from jax.sharding import PartitionSpec as P

MESH = pl.DeviceIdType.MESH


def place(n, q):
    s, t = lax.axis_index("sp"), lax.axis_index("tp")
    sibling = t + 1 - 2 * lax.rem(t, 2)
    return s, t, sibling


def greet(n, q):
    s, t, sibling = place(n, q)
    barrier = pltpu.get_barrier_semaphore()
    for i in range(1, n):
        pl.semaphore_signal(
            barrier, inc=1, device_id=(lax.rem(s + i, n), t), device_id_type=MESH
        )
    for d in range(1, q // 2):
        pl.semaphore_signal(
            barrier, inc=1, device_id=(s, lax.rem(t + 2 * d, q)), device_id_type=MESH
        )
    pl.semaphore_signal(barrier, inc=1, device_id=(s, sibling), device_id_type=MESH)
    return barrier, n - 1 + q // 2


def remote(src, dst, send_sem, recv_sem, device):
    return pltpu.make_async_remote_copy(
        src_ref=src,
        dst_ref=dst,
        send_sem=send_sem,
        recv_sem=recv_sem,
        device_id=device,
        device_id_type=MESH,
    )


def dispatch_kernel(
    n, q, ids_ref, w_ref, x_ref, g_ref, xo_ref, do_ref, p_ref,
    p01, send, buf, out_sem, s1, r1, sy, ry, ss, rs,
):
    s, t, sibling = place(n, q)
    ny = q // 2
    tok, cols = x_ref.shape
    total = send.shape[1]
    cap = total // n
    barrier, greeted = greet(n, q)

    ids0, ids1 = ids_ref[0:1, :], ids_ref[1:2, :]
    experts = lax.broadcasted_iota(jnp.int32, (n, tok), 0)
    named = jnp.logical_or(ids0 == experts, ids1 == experts)
    named_f = jnp.where(named, 1.0, 0.0)
    earlier = jnp.where(
        lax.broadcasted_iota(jnp.int32, (tok, tok), 0)
        < lax.broadcasted_iota(jnp.int32, (tok, tok), 1),
        1.0,
        0.0,
    )
    before = jnp.dot(
        named_f.astype(jnp.bfloat16),
        earlier.astype(jnp.bfloat16),
        preferred_element_type=jnp.float32,
    ).astype(jnp.int32)
    slots = lax.broadcasted_iota(jnp.int32, (cap, tok), 0)
    for e in range(n):
        here = before[e : e + 1, :] == slots
        c0 = jnp.where(jnp.logical_and(here, ids0 == e), 1.0, 0.0)
        c1 = jnp.where(jnp.logical_and(here, ids1 == e), 1.0, 0.0)
        rows = slice(e * cap, (e + 1) * cap)
        p01[rows, 0:tok] = c0.astype(jnp.bfloat16)
        p01[rows, tok : 2 * tok] = c1.astype(jnp.bfloat16)
        p_ref[rows, :] = (c0 + c1).astype(jnp.bfloat16)
    grad = g_ref[...].astype(jnp.float32)
    weighted = jnp.concatenate(
        [
            (w_ref[:, 0:1] * grad).astype(jnp.bfloat16),
            (w_ref[:, 1:2] * grad).astype(jnp.bfloat16),
        ],
        axis=0,
    )
    send[0] = jnp.dot(p_ref[...], x_ref[...], preferred_element_type=jnp.float32).astype(
        jnp.bfloat16
    )
    send[1] = jnp.dot(p01[...], weighted, preferred_element_type=jnp.float32).astype(jnp.bfloat16)

    def at_rows(j):
        return pl.ds(pl.multiple_of(j * cap, cap), cap)

    def block(j, tt):
        return buf.at[:, at_rows(j), pl.ds(pl.multiple_of(tt * cols, cols), cols)]

    def first(i):
        e = lax.rem(s + i, n)
        return remote(send.at[:, at_rows(e)], block(s, t), s1.at[i], r1.at[i], (e, t))

    def across(i, d):
        j = lax.rem(s - i + n, n)
        b = block(j, t)
        return remote(b, b, sy.at[i, d - 1], ry.at[i, d - 1], (s, lax.rem(t + 2 * d, q)))

    def beside(i, d):
        j = lax.rem(s - i + n, n)
        b = block(j, lax.rem(t - 2 * d + q, q))
        return remote(b, b, ss.at[i, d], rs.at[i, d], (s, sibling))

    pl.semaphore_wait(barrier, greeted)
    own = pltpu.make_async_copy(send.at[:, at_rows(s)], block(s, t), s1.at[0])
    own.start()
    for i in range(1, n):
        first(i).start()

    def forward(i):
        for d in range(1, ny):
            across(i, d).wait_recv()
            beside(i, d).start()

    outs = []

    def drain(i):
        j = lax.rem(s - i + n, n)
        for d in range(ny):
            beside(i, d).wait_recv()
        for a, ref in enumerate((xo_ref, do_ref)):
            copy = pltpu.make_async_copy(
                buf.at[a, at_rows(j)], ref.at[at_rows(j)], out_sem.at[i, a]
            )
            copy.start()
            outs.append(copy)

    for i in range(n):
        if i == 0:
            own.wait()
        else:
            first(i).wait_recv()
        for d in range(1, ny):
            across(i, d).start()
        beside(i, 0).start()
        if i >= 1:
            forward(i - 1)
        if i >= 2:
            drain(i - 2)
    forward(n - 1)
    for i in range(max(n - 2, 0), n):
        drain(i)
    for i in range(n):
        if i:
            first(i).wait_send()
        for d in range(1, ny):
            across(i, d).wait_send()
        for d in range(ny):
            beside(i, d).wait_send()
    for copy in outs:
        copy.wait()


def dispatch(n, q, ids_t, weight, x, g):
    tok, cols = x.shape
    total = 4 * tok
    ny = q // 2
    vmem = pl.BlockSpec(memory_space=pltpu.VMEM)
    hbm = pl.BlockSpec(memory_space=pl.ANY)
    dma = pltpu.SemaphoreType.DMA
    rows = jax.ShapeDtypeStruct((total, q * cols), jnp.bfloat16)
    return pl.pallas_call(
        functools.partial(dispatch_kernel, n, q),
        out_shape=(rows, rows, jax.ShapeDtypeStruct((total, tok), jnp.bfloat16)),
        in_specs=[vmem] * 4,
        out_specs=(hbm, hbm, vmem),
        scratch_shapes=[
            pltpu.VMEM((total, 2 * tok), jnp.bfloat16),
            pltpu.VMEM((2, total, cols), jnp.bfloat16),
            pltpu.VMEM((2, total, q * cols), jnp.bfloat16),
            dma((n, 2)),
            dma((n,)),
            dma((n,)),
            dma((n, max(ny - 1, 1))),
            dma((n, max(ny - 1, 1))),
            dma((n, ny)),
            dma((n, ny)),
        ],
        compiler_params=pltpu.CompilerParams(collective_id=0, has_side_effects=True),
        name="dispatch",
    )(ids_t, weight, x, g)


def combine_kernel(
    n, q, part_ref, p_ref, g_ref, b_ref, co_ref, c_ref, v_ref, taps_ref, w_hbm,
    x_hbm, dy_hbm, hid_hbm, dg_hbm, du_hbm,
    gout_ref, gb_ref, gc_ref, gv_ref, ggate_hbm, gup_hbm, gdown_hbm,
    rsib, pair, ryb, fin, ret, full_h, h_t, all_t, all_m, w_ref, edge, got, padded,
    x_v, dy_v, hid_v, dg_v, du_v, ggate_v, gup_v, gdown_v, in_sem, o_sem, w_sem,
    ss, rs, sy, ry, s3, r3, sm, rm, sp, rp, shy, rhy, shs, rhs, sa, ra, se, re,
):
    s, t, sibling = place(n, q)
    partner = s + 1 - 2 * lax.rem(s, 2)
    ny = q // 2
    tok, cols = g_ref.shape
    total, width = part_ref.shape
    cap = total // n
    share = width // n
    barrier, greeted = greet(n, q)
    w_copy = pltpu.make_async_copy(w_hbm, w_ref, w_sem)
    loads = [
        pltpu.make_async_copy(source, target, in_sem.at[k])
        for k, (source, target) in enumerate(
            zip((hid_hbm, dy_hbm, x_hbm, dg_hbm, du_hbm), (hid_v, dy_v, x_v, dg_v, du_v))
        )
    ]
    w_copy.start()
    for load in loads:
        load.start()
    all_m[s] = (b_ref[...].astype(jnp.float32) * co_ref[...].astype(jnp.float32)).astype(
        jnp.bfloat16
    )

    def at_rows(j):
        return pl.ds(pl.multiple_of(j * cap, cap), cap)

    def at_cols(tt):
        return pl.ds(pl.multiple_of(tt * cols, cols), cols)

    def beside(i, d):
        j = lax.rem(s + i, n)
        theirs = lax.rem(sibling + 2 * d, q)
        return remote(
            part_ref.at[at_rows(j), at_cols(theirs)],
            rsib.at[d, at_rows(j)],
            ss.at[i, d],
            rs.at[i, d],
            (s, sibling),
        )

    def across(i, d):
        j = lax.rem(s + i, n)
        return remote(
            pair.at[d - 1, at_rows(j)],
            ryb.at[d - 1, at_rows(j)],
            sy.at[i, d - 1],
            ry.at[i, d - 1],
            (s, lax.rem(t + 2 * d, q)),
        )

    def back(i):
        j = lax.rem(s + i, n)
        return remote(fin.at[at_rows(j)], ret.at[at_rows(s)], s3.at[i], r3.at[i], (j, t))

    def mixed_far(i):
        return remote(
            all_m.at[s], all_m.at[s], sm.at[i // 2], rm.at[i // 2], (lax.rem(s + i, n), t)
        )

    def mixed_near(i):
        b = all_m.at[lax.rem(s - i + n, n)]
        return remote(b, b, sp.at[i // 2], rp.at[i // 2], (partner, t))

    def h_across(d):
        b = full_h.at[:, at_cols(t)]
        return remote(b, b, shy.at[d - 1], rhy.at[d - 1], (s, lax.rem(t + 2 * d, q)))

    def h_beside(d):
        b = full_h.at[:, at_cols(lax.rem(t - 2 * d + q, q))]
        return remote(b, b, shs.at[d], rhs.at[d], (s, sibling))

    def h_share(j):
        return pl.ds(pl.multiple_of(j * share, share), share)

    def h_far(i):
        j = lax.rem(s + i, n)
        return remote(h_t.at[h_share(j)], all_t.at[s], sa.at[i], ra.at[i], (j, t))

    def halo(k):
        there = lax.rem(s + 1, n) if k == 0 else lax.rem(s - 1 + n, n)
        return remote(edge.at[k], got.at[k], se.at[k], re.at[k], (there, t))

    plain = (((1,), (0,)), ((), ()))
    stores = [
        pltpu.make_async_copy(source, target, o_sem.at[k])
        for k, (source, target) in enumerate(
            zip((gdown_v, ggate_v, gup_v), (gdown_hbm, ggate_hbm, gup_hbm))
        )
    ]

    def grad_step(left, right, target):
        def step(k, _):
            here = at_cols(k)
            target[:, here] = lax.dot_general(
                left[...], right[:, here], plain, preferred_element_type=jnp.float32
            ).astype(jnp.bfloat16)
            return 0

        return step

    def mine(j, d):
        value = part_ref[at_rows(j), at_cols(lax.rem(t + 2 * d, q))].astype(jnp.float32)
        return value + rsib[d, at_rows(j), :].astype(jnp.float32)

    order = [i % n for i in range(1, n + 1)]
    pl.semaphore_wait(barrier, greeted)
    for i in order:
        for d in [*range(1, ny), 0]:
            beside(i, d).start()
    for i in range(2, n, 2):
        mixed_far(i).start()
    mixed_near(0).start()

    def finish(i):
        j = lax.rem(s + i, n)
        beside(i, 0).wait_recv()
        value = mine(j, 0)
        for d in range(1, ny):
            across(i, d).wait_recv()
            value = value + ryb[d - 1, at_rows(j), :].astype(jnp.float32)
        value = value.astype(jnp.bfloat16)
        if i == 0:
            ret[at_rows(s), :] = value
        else:
            fin[at_rows(j), :] = value
            back(i).start()

    for k, i in enumerate(order):
        j = lax.rem(s + i, n)
        for d in range(1, ny):
            beside(i, d).wait_recv()
            pair[d - 1, at_rows(j), :] = mine(j, d).astype(jnp.bfloat16)
            across(i, d).start()
        if k >= 1:
            finish(order[k - 1])
    finish(order[-1])
    for i in range(2, n, 2):
        mixed_far(i).wait_recv()
        mixed_near(i).start()
    for load in loads:
        load.wait()
    lax.fori_loop(0, q, grad_step(hid_v, dy_v, gdown_v), 0)
    stores[0].start()
    for i in range(1, n):
        back(i).wait_recv()
    moe = lax.dot_general(
        p_ref[...], ret[...], (((0,), (0,)), ((), ())), preferred_element_type=jnp.float32
    )
    full_h[:, at_cols(t)] = (g_ref[...].astype(jnp.float32) + moe).astype(jnp.bfloat16)
    for d in range(1, ny):
        h_across(d).start()
    h_beside(0).start()
    w_copy.wait()
    for d in range(1, ny):
        h_across(d).wait_recv()
        h_beside(d).start()
    for d in range(ny):
        h_beside(d).wait_recv()
    for k in range(q):
        here = slice(k * cols, (k + 1) * cols)
        h_t[here, :] = full_h[:, here].astype(jnp.float32).T.astype(jnp.bfloat16)
    for i in range(1, n):
        h_far(i).start()
    all_t[s] = h_t[h_share(s), :]
    grad_z = jnp.dot(full_h[...], w_ref[...], preferred_element_type=jnp.float32)
    dconv = (grad_z * b_ref[...].astype(jnp.float32)).astype(jnp.bfloat16).astype(jnp.float32)
    edge[0] = jnp.broadcast_to(dconv[tok - 1 : tok, :], (8, cols))
    edge[1] = jnp.broadcast_to(dconv[0:1, :], (8, cols))
    halo(0).start()
    halo(1).start()
    gb_ref[...] = (grad_z * co_ref[...].astype(jnp.float32)).astype(jnp.bfloat16)
    padded[8 : 8 + tok, :] = dconv
    halo(0).wait_recv()
    halo(1).wait_recv()
    padded[0:8, :] = jnp.where(s > 0, got[0], 0.0)
    padded[8 + tok : 16 + tok, :] = jnp.where(s < n - 1, got[1], 0.0)
    grad_u = (
        taps_ref[0:1, :] * padded[9 : 9 + tok, :]
        + taps_ref[1:2, :] * padded[8 : 8 + tok, :]
        + taps_ref[2:3, :] * padded[7 : 7 + tok, :]
    )
    gc_ref[...] = (grad_u * v_ref[...].astype(jnp.float32)).astype(jnp.bfloat16)
    gv_ref[...] = (grad_u * c_ref[...].astype(jnp.float32)).astype(jnp.bfloat16)
    lax.fori_loop(0, q, grad_step(dg_v, x_v, ggate_v), 0)
    stores[1].start()
    lax.fori_loop(0, q, grad_step(du_v, x_v, gup_v), 0)
    stores[2].start()
    for i in range(0, n, 2):
        mixed_near(i).wait_recv()
    for i in range(1, n):
        h_far(i).wait_recv()
    total_out = jnp.zeros((share, cols), jnp.float32)
    for k in range(n):
        total_out = total_out + jnp.dot(all_t[k], all_m[k], preferred_element_type=jnp.float32)
    gout_ref[...] = total_out
    for i in range(n):
        if i:
            back(i).wait_send()
            h_far(i).wait_send()
        if i % 2 == 0:
            mixed_near(i).wait_send()
            if i:
                mixed_far(i).wait_send()
        for d in range(1, ny):
            across(i, d).wait_send()
        for d in range(ny):
            beside(i, d).wait_send()
    for d in range(ny):
        if d:
            h_across(d).wait_send()
        h_beside(d).wait_send()
    halo(0).wait_send()
    halo(1).wait_send()
    for store in stores:
        store.wait()


def combine(
    n, q, part, p, g, gate_b, conv_out, gate_c, value_v, taps, out_proj, x, dy, hid, dg, du
):
    total, width = part.shape
    tok, cols = g.shape
    share = width // n
    ny = q // 2
    far = max(ny - 1, 1)
    vmem = pl.BlockSpec(memory_space=pltpu.VMEM)
    dma = pltpu.SemaphoreType.DMA
    half = jnp.bfloat16
    like = jax.ShapeDtypeStruct(g.shape, half)
    hbm = pl.BlockSpec(memory_space=pl.ANY)
    units = hid.shape[0]
    tall = (units, width)
    sems = [(n, ny), (n, far), (n,), (n // 2,), (n // 2,), (far,), (ny,), (n,), (2,)]
    return pl.pallas_call(
        functools.partial(combine_kernel, n, q),
        out_shape=(
            jax.ShapeDtypeStruct((share, cols), jnp.float32),
            like,
            like,
            like,
            jax.ShapeDtypeStruct(tall, half),
            jax.ShapeDtypeStruct(tall, half),
            jax.ShapeDtypeStruct(tall, half),
        ),
        in_specs=[vmem] * 8 + [hbm] * 6,
        out_specs=(vmem,) * 4 + (hbm,) * 3,
        scratch_shapes=[
            pltpu.VMEM((ny, total, cols), half),
            pltpu.VMEM((far, total, cols), half),
            pltpu.VMEM((far, total, cols), half),
            pltpu.VMEM((total, cols), half),
            pltpu.VMEM((total, cols), half),
            pltpu.VMEM((tok, width), half),
            pltpu.VMEM((width, tok), half),
            pltpu.VMEM((n, share, tok), half),
            pltpu.VMEM((n, tok, cols), half),
            pltpu.VMEM(out_proj.shape, half),
            pltpu.VMEM((2, 8, cols), jnp.float32),
            pltpu.VMEM((2, 8, cols), jnp.float32),
            pltpu.VMEM((tok + 16, cols), jnp.float32),
            pltpu.VMEM((total, width), half),
            pltpu.VMEM((total, width), half),
            pltpu.VMEM((units, total), half),
            pltpu.VMEM((units, total), half),
            pltpu.VMEM((units, total), half),
            pltpu.VMEM(tall, half),
            pltpu.VMEM(tall, half),
            pltpu.VMEM(tall, half),
            dma((5,)),
            dma((3,)),
            dma,
        ]
        + [dma(shape) for shape in sems for _ in range(2)],
        compiler_params=pltpu.CompilerParams(collective_id=1, has_side_effects=True, vmem_limit_bytes=30 * 2**20),
        name="combine",
    )(part, p, g, gate_b, conv_out, gate_c, value_v, taps, out_proj, x, dy, hid, dg, du)


def local(
    out_grad,
    moe_input,
    route_weight,
    route_ids,
    gate_proj,
    up_proj,
    down_proj,
    out_proj,
    conv_out,
    gate_b,
    gate_c,
    value_v,
    conv_taps,
):
    n = lax.axis_size("sp")
    q = lax.axis_size("tp")
    xin, dyin, slots = dispatch(n, q, route_ids.T, route_weight, moe_input, out_grad)
    w_gate = gate_proj[0]
    w_up = up_proj[0]
    w_down = down_proj[0]
    gate = jnp.dot(xin, w_gate, preferred_element_type=jnp.float32)
    upval = jnp.dot(xin, w_up, preferred_element_type=jnp.float32)
    sig = jax.nn.sigmoid(gate)
    act = gate * sig
    hidden = (act * upval).astype(jnp.bfloat16)
    dhid = jnp.dot(dyin, w_down.T, preferred_element_type=jnp.float32)
    dgate = (dhid * upval * (sig * (1.0 + gate * (1.0 - sig)))).astype(jnp.bfloat16)
    dup = (dhid * act).astype(jnp.bfloat16)
    partial_value = jnp.dot(dgate, w_gate.T, preferred_element_type=jnp.float32) + jnp.dot(
        dup, w_up.T, preferred_element_type=jnp.float32
    )
    grad_out, grad_b, grad_c, grad_v, grad_gate, grad_up, grad_down = combine(
        n,
        q,
        partial_value.astype(jnp.bfloat16),
        slots,
        out_grad,
        gate_b,
        conv_out,
        gate_c,
        value_v,
        conv_taps,
        out_proj,
        xin,
        dyin,
        hidden.T,
        dgate.T,
        dup.T,
    )
    return (grad_gate.T[None], grad_up.T[None], grad_down[None], grad_out, grad_b, grad_c, grad_v)


def solution(mesh):
    in_specs = (
        P("sp", "tp"),
        P("sp", "tp"),
        P("sp", None),
        P("sp", None),
        P("sp", None, "tp"),
        P("sp", None, "tp"),
        P("sp", "tp", None),
        P(None, "tp"),
        P("sp", "tp"),
        P("sp", "tp"),
        P("sp", "tp"),
        P("sp", "tp"),
        P(None, "tp"),
    )
    out_specs = (
        P("sp", None, "tp"),
        P("sp", None, "tp"),
        P("sp", "tp", None),
        P("sp", "tp"),
        P("sp", "tp"),
        P("sp", "tp"),
        P("sp", "tp"),
    )
    return jax.shard_map(local, mesh=mesh, in_specs=in_specs, out_specs=out_specs, check_vma=False)
```

profile of v0, /device:TPU:0, one launch (start us, length us, event | category | flops | bytes accessed | tf_op | source)
XLA Modules:
  0.0 120.9 jit_solution(14930777201097683842)
XLA Ops:
  0.6 0.0 copy-start
  0.6 1.6 %copy.20.w_ref = f32[128,2]{1,0:T(8,128)} copy(f32[128,2]{0,1:T(2,128)} %param.15) | data formatting | bytes 2048 | tf_op args[2]
  2.2 40.6 %dispatch.1 = (bf16[512,2048]{1,0:T(8,128)(2,1)}, bf16[512,2048]{1,0:T(8,128)(2,1)}, bf16[512,128]{1,0:T(8,128)(2,1)}) custom-call(s32[2,128]{1,0:T(2,128)} %bitcast.67, f32[128,2]{1,0:T(8,128)} %copy.20.w_ref, bf16[128,512]{1,0:T(8,128)(2,1)} %x_ref.1, bf16[128,512]{1,0:T(8,128)(2,1)} %g_ref.3), custom_call_target="tpu_custom_call" | custom-call | tf_op jit(solution)/shard_map/dispatch/pallas_call | solution.py:171
  42.8 0.0 copy-start.12
  42.8 4.3 %fusion.2 = f32[512,704]{0,1:T(8,128)S(1)} fusion(bf16[512,2048]{1,0:T(8,128)(2,1)} %get-tuple-element.18.x_hbm, bf16[1,2048,704]{1,2,0:T(8,128)(2,1)} %param.17), kind=kOutput, calls=%fused_computation.3 | convolution fusion | flops 1476395008 | bytes 6422528 | tf_op jit(solution)/shard_map/dot_general | solution.py:499
  47.1 1.7 %fusion.5 = f32[512,704]{0,1:T(8,128)S(1)} fusion(bf16[512,2048]{1,0:T(8,128)(2,1)S(1)} %copy-done.2, bf16[1,2048,704]{1,2,0:T(8,128)(2,1)S(1)} %copy-done.12), kind=kOutput, calls=%fused_computation.6 | convolution fusion | flops 1476395008 | bytes 6422528 | tf_op jit(solution)/shard_map/dot_general | solution.py:500
  48.9 0.0 copy-start.11
  48.9 2.2 %fusion.11 = (bf16[704,512]{1,0:T(8,128)(2,1)S(1)}, bf16[704,512]{1,0:T(8,128)(2,1)S(1)}, bf16[704,512]{1,0:T(8,128)(2,1)S(1)}, f32[512,704]{0,1:T(8,128)S(1)}) fusion(f32[512,704]{0,1:T(8,128)S(1)} %fusion.2, f32[512,704]{0,1:T(8,128)S(1)} %fusion.5, bf16[512,2048]{1,0:T(8,128)(2,1)S(1)} %copy-done.3, bf16[1,704,2048]{2,1,0:T(8,128)(2,1)S(1)} %copy-done), kind=kOutput, calls=%fused_computation.14 | convolution fusion | flops 1481801728 | bytes 11468800 | tf_op jit(solution)/shard_map/dot_general | solution.py:504
  51.1 2.2 %fusion = f32[512,2048]{1,0:T(8,128)S(1)} fusion(bf16[1,2048,704]{1,2,0:T(8,128)(2,1)S(1)} %copy-done.11, f32[512,704]{0,1:T(8,128)S(1)} %fusion.2, f32[512,704]{0,1:T(8,128)S(1)} %get-tuple-element.30, f32[512,704]{0,1:T(8,128)S(1)} %fusion.5), kind=kOutput, calls=%fused_computation.1 | convolution fusion | flops 1479999488 | bytes 11403264 | tf_op jit(solution)/shard_map/dot_general | solution.py:507
  53.3 0.0 copy-start.1
  53.3 0.0 copy-start.4
  53.3 0.0 copy-start.5
  53.3 0.0 copy-start.6
  53.3 0.0 copy-start.7
  53.3 0.0 copy-start.8
  53.4 2.1 %add_convert_fusion.part_ref = bf16[512,2048]{1,0:T(8,128)(2,1)S(1)} fusion(f32[512,2048]{1,0:T(8,128)S(1)} %fusion, bf16[1,2048,704]{1,2,0:T(8,128)(2,1)S(1)} %copy-done.12, f32[512,704]{0,1:T(8,128)S(1)} %get-tuple-element.30, f32[512,704]{0,1:T(8,128)S(1)} %fusion.2), kind=kOutput, calls=%fused_computation | convolution fusion | flops 1480654848 | bytes 12058624 | tf_op jit(solution)/shard_map/dot_general | solution.py:507
  55.5 57.9 %combine.1 = (f32[256,512]{1,0:T(8,128)S(1)}, bf16[128,512]{1,0:T(8,128)(2,1)S(1)}, bf16[128,512]{1,0:T(8,128)(2,1)S(1)}, bf16[128,512]{1,0:T(8,128)(2,1)S(1)}, ...) custom-call(bf16[512,2048]{1,0:T(8,128)(2,1)S(1)} %add_convert_fusion.part_ref, ...), custom_call_target="tpu_custom_call" | custom-call | tf_op jit(solution)/shard_map/combine/pallas_call | solution.py:433
  113.4 1.6 %copy.28 = bf16[1,2048,704]{1,2,0:T(8,128)(2,1)} copy(bf16[1,2048,704]{1,2,0:T(8,128)(2,1)S(1)} %bitcast.66) | data formatting | bytes 5767168
  115.0 1.6 %copy.29 = bf16[1,2048,704]{1,2,0:T(8,128)(2,1)} copy(bf16[1,2048,704]{1,2,0:T(8,128)(2,1)S(1)} %bitcast.65) | data formatting | bytes 5767168
  116.6 1.6 %copy.30 = bf16[1,704,2048]{2,1,0:T(8,128)(2,1)} copy(bf16[1,704,2048]{2,1,0:T(8,128)(2,1)S(1)} %bitcast.64) | data formatting | bytes 5767168
  118.1 0.8 copy.31
  118.9 0.7 copy.32
  119.6 0.7 copy.33
  120.2 0.7 copy.34
  (17 shorter events, 0.0 us)
Async XLA Ops:
  0.6 48.2 %copy-start = (bf16[1,704,2048]{2,1,0:T(8,128)(2,1)S(1)}, bf16[1,704,2048]{2,1,0:T(8,128)(2,1)}, u32[]{:S(2)}) copy-start(bf16[1,704,2048]{2,1,0:T(8,128)(2,1)} %param.19) | copy-start | bytes 8650756
  42.8 4.3 %copy-start.2 = (bf16[512,2048]{1,0:T(8,128)(2,1)S(1)}, bf16[512,2048]{1,0:T(8,128)(2,1)}, u32[]{:S(2)}) copy-start(bf16[512,2048]{1,0:T(8,128)(2,1)} %get-tuple-element.18.x_hbm) | copy-start | bytes 6291460
  42.8 4.3 %copy-start.12 = (bf16[1,2048,704]{1,2,0:T(8,128)(2,1)S(1)}, bf16[1,2048,704]{1,2,0:T(8,128)(2,1)}, u32[]{:S(2)}) copy-start(bf16[1,2048,704]{1,2,0:T(8,128)(2,1)} %param.18) | copy-start | bytes 8650756
  47.1 1.7 %copy-start.3 = (bf16[512,2048]{1,0:T(8,128)(2,1)S(1)}, bf16[512,2048]{1,0:T(8,128)(2,1)}, u32[]{:S(2)}) copy-start(bf16[512,2048]{1,0:T(8,128)(2,1)} %get-tuple-element.17.dy_hbm) | copy-start | bytes 6291460
  48.9 2.2 %copy-start.11 = (bf16[1,2048,704]{1,2,0:T(8,128)(2,1)S(1)}, bf16[1,2048,704]{1,2,0:T(8,128)(2,1)}, u32[]{:S(2)}) copy-start(bf16[1,2048,704]{1,2,0:T(8,128)(2,1)} %param.17) | copy-start | bytes 8650756
  53.3 2.2 %copy-start.1 = (bf16[2048,512]{1,0:T(8,128)(2,1)S(1)}, bf16[2048,512]{1,0:T(8,128)(2,1)}, u32[]{:S(2)}) copy-start(bf16[2048,512]{1,0:T(8,128)(2,1)} %w_hbm.1) | copy-start | bytes 6291460
  53.3 2.2 %copy-start.4 = (bf16[128,512]{1,0:T(8,128)(2,1)S(1)}, bf16[128,512]{1,0:T(8,128)(2,1)}, u32[]{:S(2)}) copy-start(bf16[128,512]{1,0:T(8,128)(2,1)} %g_ref.3) | copy-start | bytes 393220
  53.3 2.2 %copy-start.5 = (bf16[128,512]{1,0:T(8,128)(2,1)S(1)}, bf16[128,512]{1,0:T(8,128)(2,1)}, u32[]{:S(2)}) copy-start(bf16[128,512]{1,0:T(8,128)(2,1)} %b_ref.1) | copy-start | bytes 393220
  53.3 2.2 %copy-start.6 = (bf16[128,512]{1,0:T(8,128)(2,1)S(1)}, bf16[128,512]{1,0:T(8,128)(2,1)}, u32[]{:S(2)}) copy-start(bf16[128,512]{1,0:T(8,128)(2,1)} %co_ref.1) | copy-start | bytes 393220
  53.3 2.2 %copy-start.7 = (bf16[128,512]{1,0:T(8,128)(2,1)S(1)}, bf16[128,512]{1,0:T(8,128)(2,1)}, u32[]{:S(2)}) copy-start(bf16[128,512]{1,0:T(8,128)(2,1)} %c_ref.1) | copy-start | bytes 393220
  53.3 2.1 %copy-start.8 = (bf16[128,512]{1,0:T(8,128)(2,1)S(1)}, bf16[128,512]{1,0:T(8,128)(2,1)}, u32[]{:S(2)}) copy-start(bf16[128,512]{1,0:T(8,128)(2,1)} %v_ref.1) | copy-start | bytes 393220
  53.3 2.1 %copy-start.9 = (bf16[512,128]{1,0:T(8,128)(2,1)S(1)}, bf16[512,128]{1,0:T(8,128)(2,1)}, u32[]{:S(2)}) copy-start(bf16[512,128]{1,0:T(8,128)(2,1)} %get-tuple-element.19.p_ref) | copy-start | bytes 393220
  53.4 2.1 %copy-start.10 = (f32[3,512]{1,0:T(4,128)S(1)}, f32[3,512]{1,0:T(4,128)}, u32[]{:S(2)}) copy-start(f32[3,512]{1,0:T(4,128)} %taps_ref.1) | copy-start | bytes 18436
where the time goes:
time: 121 us
  Pallas kernels  98.5 us (81%)
  matrix products  12.4 us (10%)
  local copies, waits for them, and re-layouts  9.14 us (8%)
    pallas_call x1, Pallas kernels, combine(): pl.pallas_call(functools.partial(combine_kernel, n, q), out_shape=(jax.Sh...  57.9 us
    pallas_call x1, Pallas kernels, dispatch(): pl.pallas_call(functools.partial(dispatch_kernel, n, q), out_shape=(rows,...  40.6 us
    unnamed x34, local copies, waits for them, and re-layouts  9.14 us
    dot_general x1, matrix products, local(): gate = jnp.dot(xin, w_gate, preferred_element_type=jnp.float32)  4.28 us

commit v1 on v0

v1 whole, which is shorter than its diff:
```python
import functools

import jax
import jax.numpy as jnp
from jax import lax
from jax.experimental import pallas as pl
from jax.experimental.pallas import tpu as pltpu
from jax.sharding import PartitionSpec as P

MESH = pl.DeviceIdType.MESH
HALF = jnp.bfloat16
F32 = jnp.float32
PLAIN = (((1,), (0,)), ((), ()))
RIGHT_T = (((1,), (1,)), ((), ()))


def remote(src, dst, send_sem, recv_sem, device):
    return pltpu.make_async_remote_copy(
        src_ref=src,
        dst_ref=dst,
        send_sem=send_sem,
        recv_sem=recv_sem,
        device_id=device,
        device_id_type=MESH,
    )


def offsets(n):
    m = n // 2
    shifts = [0] + sorted(range(1, m), key=lambda k: -min(k, m - k))
    return [(k, f) for k in shifts for f in range(2)]


def layer_kernel(
    n, q,
    ids_hbm, rw_hbm, x_hbm, g_hbm, b_hbm, co_hbm, c_hbm, v_hbm, taps_hbm,
    wg_hbm, wu_hbm, wd_hbm, wo_hbm,
    gout_ref, gb_ref, gc_ref, gv_ref, ggate_ref, gup_ref, gdown_ref,
    ids_ref, rw_ref, x_ref, g_ref, b_ref, co_ref, c_ref, v_ref, taps_ref,
    wg, wu, wd, wo, p01, p_ref, p_t, send, buf, gate, upval, dhid, hid, dg, du, turned,
    part, rsib, pair, ryb, fin, ret, full_h, h_t, all_t, all_m, edge, got, padded,
    w_sem,
    s1, r1, sy, ry, ss, rs, s2, r2, s3, r3, s4, r4,
    sm, rm, sp, rp, shy, rhy, shs, rhs, sa, ra, sf, rf, se, re,
):
    s, t = lax.axis_index("sp"), lax.axis_index("tp")
    core = lax.rem(t, 2)
    sibling = t + 1 - 2 * core
    partner = s + 1 - 2 * lax.rem(s, 2)
    ny = q // 2
    tok, cols = x_ref.shape
    total, width = part.shape
    cap = total // n
    share = width // n
    units = wg.shape[0]
    pairs = offsets(n)
    batch = total // 2
    mid = n // 2

    barrier = pltpu.get_barrier_semaphore()
    for i in range(1, n):
        pl.semaphore_signal(
            barrier, inc=1, device_id=(lax.rem(s + i, n), t), device_id_type=MESH
        )
    for d in range(1, ny):
        pl.semaphore_signal(
            barrier, inc=1, device_id=(s, lax.rem(t + 2 * d, q)), device_id_type=MESH
        )
    pl.semaphore_signal(barrier, inc=1, device_id=(s, sibling), device_id_type=MESH)

    loads = [
        pltpu.make_async_copy(source, target, w_sem.at[k])
        for k, (source, target) in enumerate(
            zip(
                (
                    wg_hbm, wu_hbm, wd_hbm, wo_hbm, ids_hbm, x_hbm, rw_hbm, g_hbm,
                    b_hbm, co_hbm, c_hbm, v_hbm, taps_hbm,
                ),
                (
                    wg, wu, wd, wo, ids_ref, x_ref, rw_ref, g_ref,
                    b_ref, co_ref, c_ref, v_ref, taps_ref,
                ),
            )
        )
    ]
    for load in [*loads[4:], *loads[:4]]:
        load.start()

    def to(p):
        k, f = pairs[p]
        return lax.rem((partner if f else s) + 2 * k, n)

    def source(p):
        k, f = pairs[p]
        return lax.rem((partner if f else s) - 2 * k + n, n)

    def rows(p):
        return slice(p * cap, (p + 1) * cap)

    def at_cols(tt):
        return pl.ds(pl.multiple_of(tt * cols, cols), cols)

    loads[4].wait()
    ids0, ids1 = ids_ref[0:1, :], ids_ref[1:2, :]
    where = lax.broadcasted_iota(jnp.int32, (n, tok), 0)
    experts = jnp.zeros((n, tok), jnp.int32)
    for p in range(n):
        experts = jnp.where(where == p, to(p), experts)
    named = jnp.logical_or(ids0 == experts, ids1 == experts)
    row_i = lax.broadcasted_iota(jnp.int32, (tok, tok), 0)
    col_i = lax.broadcasted_iota(jnp.int32, (tok, tok), 1)
    before = jnp.dot(
        jnp.where(named, 1.0, 0.0).astype(HALF),
        jnp.where(row_i < col_i, 1.0, 0.0).astype(HALF),
        preferred_element_type=F32,
    ).astype(jnp.int32)
    slots = lax.broadcasted_iota(jnp.int32, (cap, tok), 0)
    for p in range(n):
        here = before[p : p + 1, :] == slots
        c0 = jnp.where(jnp.logical_and(here, ids0 == to(p)), 1.0, 0.0)
        c1 = jnp.where(jnp.logical_and(here, ids1 == to(p)), 1.0, 0.0)
        p01[rows(p), 0:tok] = c0.astype(HALF)
        p01[rows(p), tok : 2 * tok] = c1.astype(HALF)
        p_ref[rows(p), :] = (c0 + c1).astype(HALF)

    def first(a, p):
        return remote(
            send.at[a, rows(p)],
            buf.at[a, rows(p), at_cols(t)],
            s1.at[a, p],
            r1.at[a, p],
            (to(p), t),
        )

    def across(a, p, d):
        b = buf.at[a, rows(p), at_cols(t)]
        return remote(
            b, b, sy.at[a, p, d - 1], ry.at[a, p, d - 1], (s, lax.rem(t + 2 * d, q))
        )

    def beside(a, p, d):
        b = buf.at[a, rows(p), at_cols(lax.rem(t - 2 * d + q, q))]
        return remote(b, b, ss.at[a, p, d], rs.at[a, p, d], (s, sibling))

    send_order = [*range(2, n), 1]
    loads[5].wait()
    send[0] = jnp.dot(p_ref[...], x_ref[...], preferred_element_type=F32).astype(HALF)
    pl.semaphore_wait(barrier, n - 1 + ny)
    for p in send_order:
        first(0, p).start()
    buf[0, rows(0), at_cols(t)] = send[0, rows(0), :]
    loads[6].wait()
    loads[7].wait()
    grad = g_ref[...].astype(F32)
    weighted = []
    for k in range(2):
        column = jnp.sum(
            jnp.where(row_i == col_i, rw_ref[k : k + 1, :], 0.0), axis=1, keepdims=True
        )
        weighted.append((column * grad).astype(HALF))
    send[1] = jnp.dot(
        p01[...], jnp.concatenate(weighted, axis=0), preferred_element_type=F32
    ).astype(HALF)
    for p in send_order:
        first(1, p).start()
    buf[1, rows(0), at_cols(t)] = send[1, rows(0), :]

    def span(h):
        return slice(h * batch, (h + 1) * batch)

    def forward_gate(h):
        gate[span(h), :] = lax.dot_general(
            buf[0, span(h), :], wg[...], RIGHT_T, preferred_element_type=F32
        )

    def forward_up(h):
        upval[span(h), :] = lax.dot_general(
            buf[0, span(h), :], wu[...], RIGHT_T, preferred_element_type=F32
        )

    def back_hidden(h):
        dhid[span(h), :] = lax.dot_general(
            buf[1, span(h), :], wd[...], RIGHT_T, preferred_element_type=F32
        )

    step_rows = 32

    def activation(h):
        def step(r, _):
            at = pl.ds(pl.multiple_of(h * batch + r * step_rows, step_rows), step_rows)
            z, u, dh = gate[at, :], upval[at, :], dhid[at, :]
            sig = jax.nn.sigmoid(z)
            act = z * sig
            hid[at, :] = (act * u).astype(HALF)
            dg[at, :] = (dh * u * (sig * (1.0 + z * (1.0 - sig)))).astype(HALF)
            du[at, :] = (dh * act).astype(HALF)
            return 0

        lax.fori_loop(0, batch // step_rows, step, 0)

    def partial(h):
        def step(k, _):
            here = at_cols(k)
            part[span(h), here] = (
                lax.dot_general(
                    dg[span(h), :], wg[:, here], PLAIN, preferred_element_type=F32
                )
                + lax.dot_general(
                    du[span(h), :], wu[:, here], PLAIN, preferred_element_type=F32
                )
            ).astype(HALF)
            return 0

        lax.fori_loop(0, q, step, 0)

    seq = [(0, 0), (1, 0), (0, 1), (1, 1)]
    seq += [(0, p) for p in range(2, n)] + [(1, p) for p in range(2, n)]

    def last_of(a, h):
        return max(k for k, (b, p) in enumerate(seq) if b == a and p // mid == h)

    drained = set()

    def drain(upto):
        for k in range(upto + 1):
            if k not in drained:
                drained.add(k)
                for d in range(ny):
                    beside(*seq[k], d).wait_recv()

    def weights(k):
        loads[k].wait()

    def mixed_own():
        for k in range(8, 13):
            loads[k].wait()
        all_m[0:tok, :] = (b_ref[...].astype(F32) * co_ref[...].astype(F32)).astype(HALF)

    def turn_slots():
        p_t[...] = p_ref[...].astype(F32).T.astype(HALF)

    hooks = {}

    def hook(k, *calls):
        hooks.setdefault(min(k, len(seq) - 1), []).extend(calls)

    hook(1, (None, mixed_own))
    hook(2, (None, turn_slots))
    x_a, x_b = last_of(0, 0), last_of(0, 1)
    d_a, d_b = last_of(1, 0), last_of(1, 1)
    hook(x_a + 3, (x_a, lambda: (weights(0), forward_gate(0))))
    hook(x_a + 4, (x_a, lambda: (weights(1), forward_up(0))))
    hook(x_b + 3, (x_b, lambda: forward_gate(1)))
    hook(x_b + 4, (x_b, lambda: forward_up(1)))
    hook(d_a + 3, (d_a, lambda: (weights(2), back_hidden(0))))
    hook(d_a + 4, (d_a, lambda: activation(0)))

    def forward(k):
        for d in range(1, ny):
            across(*seq[k], d).wait_recv()
            beside(*seq[k], d).start()

    for k, (a, p) in enumerate(seq):
        if p:
            first(a, p).wait_recv()
        for d in range(1, ny):
            across(a, p, d).start()
        beside(a, p, 0).start()
        if k:
            forward(k - 1)
        for need, call in hooks.get(k, []):
            if need is not None:
                drain(need)
            call()

    def mixed_far(k):
        return remote(
            all_m.at[0:tok],
            all_m.at[slot_of(k, 0)],
            sm.at[k],
            rm.at[k],
            (lax.rem(s + 2 * k, n), t),
        )

    def slot_of(k, f):
        p = pairs.index((k, f))
        return slice(p * tok, (p + 1) * tok)

    def mixed_near(k):
        return remote(
            all_m.at[slot_of(k, 0)], all_m.at[slot_of(k, 1)], sp.at[k], rp.at[k], (partner, t)
        )

    def to_side(p, d):
        theirs = lax.rem(sibling + 2 * d, q)
        return remote(
            part.at[rows(p), at_cols(theirs)],
            rsib.at[d, rows(p)],
            s2.at[p, d],
            r2.at[p, d],
            (s, sibling),
        )

    def to_far(p, d):
        return remote(
            pair.at[d - 1, rows(p)],
            ryb.at[d - 1, rows(p)],
            s3.at[p, d - 1],
            r3.at[p, d - 1],
            (s, lax.rem(t + 2 * d, q)),
        )

    def back(p):
        return remote(fin.at[rows(p)], ret.at[rows(p)], s4.at[p], r4.at[p], (source(p), t))

    def mine(p, d):
        value = part[rows(p), at_cols(lax.rem(t + 2 * d, q))].astype(F32)
        return value + rsib[d, rows(p), :].astype(F32)

    def side_start(p):
        for d in [*range(1, ny), 0]:
            to_side(p, d).start()

    def pair_up(p):
        for d in range(1, ny):
            to_side(p, d).wait_recv()
            pair[d - 1, rows(p), :] = mine(p, d).astype(HALF)
            to_far(p, d).start()

    def finish(p):
        to_side(p, 0).wait_recv()
        value = mine(p, 0)
        for d in range(1, ny):
            to_far(p, d).wait_recv()
            value = value + ryb[d - 1, rows(p), :].astype(F32)
        if p:
            fin[rows(p), :] = value.astype(HALF)
            back(p).start()
        else:
            ret[rows(p), :] = value.astype(HALF)

    near_half, far_half = [*range(2, mid), 1, 0], [*range(mid, n)]
    forward(len(seq) - 1)
    shifts = [k for k, f in pairs if f == 0][1:]
    early, late = shifts[: (len(shifts) + 1) // 3], shifts[(len(shifts) + 1) // 3 :]
    for k in early:
        mixed_far(k).start()
    mixed_near(0).start()
    partial(0)
    for p in near_half:
        side_start(p)
    drain(d_b)
    back_hidden(1)
    for p in near_half[:-1]:
        pair_up(p)
    activation(1)
    finish(near_half[0])
    partial(1)
    for p in far_half:
        side_start(p)
    if len(near_half) > 2:
        finish(near_half[1])
    for p in far_half + [0]:
        pair_up(p)
    for p in near_half[2:-1] + far_half + [0]:
        finish(p)
    for k in early:
        mixed_far(k).wait_recv()
        mixed_near(k).start()
    for k in late:
        mixed_far(k).start()

    def weight_grad(left, a, target):
        turned[...] = left[...].astype(F32).T.astype(HALF)

        def step(j, _):
            here = at_cols(j)
            target[:, here] = lax.dot_general(
                turned[...], buf[a, :, here], PLAIN, preferred_element_type=F32
            ).astype(HALF)
            return 0

        lax.fori_loop(0, q, step, 0)

    weight_grad(hid, 1, gdown_ref)
    for p in range(1, n):
        back(p).wait_recv()
    moe = jnp.dot(p_t[...], ret[...], preferred_element_type=F32)
    full_h[:, at_cols(t)] = (g_ref[...].astype(F32) + moe).astype(HALF)

    def h_across(d):
        b = full_h.at[:, at_cols(t)]
        return remote(b, b, shy.at[d - 1], rhy.at[d - 1], (s, lax.rem(t + 2 * d, q)))

    def h_beside(d):
        b = full_h.at[:, at_cols(lax.rem(t - 2 * d + q, q))]
        return remote(b, b, shs.at[d], rhs.at[d], (s, sibling))

    for d in range(1, ny):
        h_across(d).start()
    h_beside(0).start()

    def turn_h(tt):
        h_t[at_cols(tt), :] = full_h[:, at_cols(tt)].astype(F32).T.astype(HALF)

    turn_h(t)
    weights(3)
    weight_grad(dg, 0, ggate_ref)
    h_beside(0).wait_recv()
    turn_h(sibling)
    for d in range(1, ny):
        h_across(d).wait_recv()
        h_beside(d).start()
        turn_h(lax.rem(t - 2 * d + q, q))
    for d in range(1, ny):
        h_beside(d).wait_recv()
        turn_h(lax.rem(sibling - 2 * d + q, q))

    part_share = share // 2

    def half_rows(first_row):
        return pl.ds(
            pl.multiple_of(first_row + core * part_share, part_share), part_share
        )

    def tokens(p):
        return slice(p * tok, (p + 1) * tok)

    def h_far(p):
        return remote(
            h_t.at[half_rows(to(p) * share)],
            all_t.at[half_rows(0), tokens(p)],
            sa.at[p],
            ra.at[p],
            (to(p), t),
        )

    def h_pass(p):
        b = all_t.at[half_rows(0), tokens(p)]
        return remote(b, b, sf.at[p], rf.at[p], (s, sibling))

    for p in send_order:
        h_far(p).start()
    all_t[:, tokens(0)] = h_t[pl.ds(pl.multiple_of(s * share, share), share), :]

    def halo(k):
        there = lax.rem(s + 1, n) if k == 0 else lax.rem(s - 1 + n, n)
        return remote(edge.at[k], got.at[k], se.at[k], re.at[k], (there, t))

    grad_z = jnp.dot(full_h[...], wo[...], preferred_element_type=F32)
    dconv = (grad_z * b_ref[...].astype(F32)).astype(HALF).astype(F32)
    edge[0] = jnp.broadcast_to(dconv[tok - 1 : tok, :], (8, cols))
    edge[1] = jnp.broadcast_to(dconv[0:1, :], (8, cols))
    halo(0).start()
    halo(1).start()
    gb_ref[...] = (grad_z * co_ref[...].astype(F32)).astype(HALF)
    padded[8 : 8 + tok, :] = dconv
    for k in late:
        mixed_far(k).wait_recv()
        mixed_near(k).start()
    weight_grad(du, 0, gup_ref)
    halo(0).wait_recv()
    halo(1).wait_recv()
    padded[0:8, :] = jnp.where(s > 0, got[0], 0.0)
    padded[8 + tok : 16 + tok, :] = jnp.where(s < n - 1, got[1], 0.0)
    grad_u = (
        taps_ref[0:1, :] * padded[9 : 9 + tok, :]
        + taps_ref[1:2, :] * padded[8 : 8 + tok, :]
        + taps_ref[2:3, :] * padded[7 : 7 + tok, :]
    )
    gc_ref[...] = (grad_u * v_ref[...].astype(F32)).astype(HALF)
    gv_ref[...] = (grad_u * c_ref[...].astype(F32)).astype(HALF)
    for p in send_order:
        h_far(p).wait_recv()
        h_pass(p).start()
    for k in [0, *early, *late]:
        mixed_near(k).wait_recv()
    for p in send_order:
        h_pass(p).wait_recv()
    gout_ref[...] = jnp.dot(all_t[...], all_m[...], preferred_element_type=F32)

    for p in range(n):
        for a in range(2):
            if p:
                first(a, p).wait_send()
            for d in range(1, ny):
                across(a, p, d).wait_send()
            for d in range(ny):
                beside(a, p, d).wait_send()
        for d in range(ny):
            to_side(p, d).wait_send()
            if d:
                to_far(p, d).wait_send()
        if p:
            back(p).wait_send()
            h_far(p).wait_send()
            h_pass(p).wait_send()
    for d in range(ny):
        if d:
            h_across(d).wait_send()
        h_beside(d).wait_send()
    for k in [0, *early, *late]:
        if k:
            mixed_far(k).wait_send()
        mixed_near(k).wait_send()
    halo(0).wait_send()
    halo(1).wait_send()


def layer(n, q, ids_t, weight_t, x, g, b, co, c, v, taps, wg, wu, wd, wo):
    tok, cols = x.shape
    units, width = wg.shape
    total = 4 * tok
    share = width // n
    ny = q // 2
    far = max(ny - 1, 1)
    vmem = pl.BlockSpec(memory_space=pltpu.VMEM)
    hbm = pl.BlockSpec(memory_space=pltpu.HBM)
    dma = pltpu.SemaphoreType.DMA
    like = pltpu.VMEM(g.shape, HALF)
    tall = pltpu.VMEM((units, width), HALF)

    def half(*shape):
        return pltpu.VMEM(shape, HALF)

    def full(*shape):
        return pltpu.VMEM(shape, F32)

    sems = [
        (2, n), (2, n, far), (2, n, ny), (n, ny), (n, far), (n,),
        (n // 2,), (n // 2,), (far,), (ny,), (n,), (n,), (2,),
    ]
    return pl.pallas_call(
        functools.partial(layer_kernel, n, q),
        out_shape=(
            pltpu.VMEM((share, cols), F32), like, like, like, tall, tall, tall,
        ),
        in_specs=[hbm] * 13,
        out_specs=(vmem,) * 7,
        scratch_shapes=[
            pltpu.VMEM(ids_t.shape, ids_t.dtype),
            full(*weight_t.shape),
            half(tok, cols),
            half(tok, cols),
            half(tok, cols),
            half(tok, cols),
            half(tok, cols),
            half(tok, cols),
            full(*taps.shape),
            half(units, width),
            half(units, width),
            half(units, width),
            half(width, cols),
            half(total, 2 * tok),
            half(total, tok),
            half(tok, total),
            half(2, total, cols),
            half(2, total, width),
            full(total, units),
            full(total, units),
            full(total, units),
            half(total, units),
            half(total, units),
            half(total, units),
            half(units, total),
            half(total, width),
            half(ny, total, cols),
            half(far, total, cols),
            half(far, total, cols),
            half(total, cols),
            half(total, cols),
            half(tok, width),
            half(width, tok),
            half(share, n * tok),
            half(n * tok, cols),
            full(2, 8, cols),
            full(2, 8, cols),
            full(tok + 16, cols),
            dma((13,)),
        ]
        + [dma(shape) for shape in sems for _ in range(2)],
        compiler_params=pltpu.CompilerParams(
            collective_id=0, has_side_effects=True, vmem_limit_bytes=44 * 2**20
        ),
        name="layer",
    )(
        *(
            pltpu.with_memory_space_constraint(a, pltpu.HBM)
            for a in (ids_t, weight_t, x, g, b, co, c, v, taps, wg, wu, wd, wo)
        )
    )


def settle_kernel(*refs):
    count = (len(refs) - 1) // 2
    sem = refs[-1]
    copies = [
        pltpu.make_async_copy(refs[k], refs[count + k], sem.at[k]) for k in range(count)
    ]
    for copy in copies:
        copy.start()
    for copy in copies:
        copy.wait()


def settle(*arrays):
    return pl.pallas_call(
        settle_kernel,
        out_shape=tuple(pltpu.HBM(a.shape, a.dtype) for a in arrays),
        in_specs=[pl.BlockSpec(memory_space=pltpu.VMEM)] * len(arrays),
        out_specs=(pl.BlockSpec(memory_space=pltpu.HBM),) * len(arrays),
        scratch_shapes=[pltpu.SemaphoreType.DMA((len(arrays),))],
        compiler_params=pltpu.CompilerParams(vmem_limit_bytes=2**20),
        name="settle",
    )(*(pltpu.with_memory_space_constraint(a, pltpu.VMEM) for a in arrays))


def local(
    out_grad,
    moe_input,
    route_weight,
    route_ids,
    gate_proj,
    up_proj,
    down_proj,
    out_proj,
    conv_out,
    gate_b,
    gate_c,
    value_v,
    conv_taps,
):
    n = lax.axis_size("sp")
    q = lax.axis_size("tp")
    results = layer(
        n, q, route_ids.T, route_weight.T, moe_input, out_grad, gate_b, conv_out, gate_c,
        value_v, conv_taps, gate_proj[0].T, up_proj[0].T, down_proj[0], out_proj,
    )
    grad_out, grad_b, grad_c, grad_v, grad_gate, grad_up, grad_down = settle(*results)
    return (grad_gate.T[None], grad_up.T[None], grad_down[None], grad_out, grad_b, grad_c, grad_v)


def solution(mesh):
    in_specs = (
        P("sp", "tp"),
        P("sp", "tp"),
        P("sp", None),
        P("sp", None),
        P("sp", None, "tp"),
        P("sp", None, "tp"),
        P("sp", "tp", None),
        P(None, "tp"),
        P("sp", "tp"),
        P("sp", "tp"),
        P("sp", "tp"),
        P("sp", "tp"),
        P(None, "tp"),
    )
    out_specs = (
        P("sp", None, "tp"),
        P("sp", None, "tp"),
        P("sp", "tp", None),
        P("sp", "tp"),
        P("sp", "tp"),
        P("sp", "tp"),
        P("sp", "tp"),
    )
    return jax.shard_map(local, mesh=mesh, in_specs=in_specs, out_specs=out_specs, check_vma=False)
```

time: 121 us -> 91.1 us (0.75)
  matrix products: 12.4 us -> 0 us
  local copies, waits for them, and re-layouts: 9.14 us -> 0 us
  Pallas kernels: 98.5 us -> 90.3 us
    dot_general x5 -> x0, matrix products: 12.4 us -> none  [the longest x1 4.28 us: local(): gate = jnp.dot(xin, w_gate, preferred_element_type=jnp.float32)]
    unnamed x34 -> x0, local copies, waits for them, and re-layouts: 9.14 us -> none
    pallas_call x2, Pallas kernels: 98.5 us -> 90.3 us  [the longest x1 86.4 us: layer(): pl.pallas_call(functools.partial(layer_kernel, n, q), out_shape=(pltpu.VM...]
where the time goes in v1:
time: 91.1 us; the launch traced here: 90.9 us
  Pallas kernels  90.3 us (99%)
    pallas_call x1, Pallas kernels, layer(): pl.pallas_call(functools.partial(layer_kernel, n, q), out_shape=(pltpu.VM...  86.4 us
    pallas_call x1, Pallas kernels, settle(): pl.pallas_call(settle_kernel, out_shape=tuple((pltpu.HBM(a.shape, a.dtype...  3.84 us

profile of v1, /device:TPU:0, one launch (start us, length us, event | category | flops | bytes accessed | tf_op | source)
XLA Modules:
  0.0 90.9 jit_solution(8237715299636008648)
XLA Ops:
  0.6 86.4 %layer.1 = (f32[256,512]{1,0:T(8,128)S(1)}, bf16[128,512]{1,0:T(8,128)(2,1)S(1)}, bf16[128,512]{1,0:T(8,128)(2,1)S(1)}, bf16[128,512]{1,0:T(8,128)(2,1)S(1)}, bf...) custom-call(s32[2,128]{1,0:T(2,128)} %bitcast.19, f32[2,128]{1,0:T(2,128)} %bitcast.20, ...), custom_call_target="tpu_custom_call" | custom-call | tf_op jit(solution)/shard_map/layer/pallas_call | solution.py:533
  87.1 3.8 %settle.1 = (f32[256,512]{1,0:T(8,128)}, bf16[128,512]{1,0:T(8,128)(2,1)}, bf16[128,512]{1,0:T(8,128)(2,1)}, bf16[128,512]{1,0:T(8,128)(2,1)}, bf16[704,2048]{1,...) custom-call(f32[256,512]{1,0:T(8,128)S(1)} %get-tuple-element.21.refs_0_, ...), custom_call_target="tpu_custom_call" | custom-call | tf_op jit(solution)/shard_map/settle/pallas_call | solution.py:607

commit v2 on v1

--- a/solution.py
+++ b/solution.py
@@ -25,37 +25,29 @@
     )
 
 
-def offsets(n):
-    m = n // 2
-    shifts = [0] + sorted(range(1, m), key=lambda k: -min(k, m - k))
-    return [(k, f) for k in shifts for f in range(2)]
-
-
 def layer_kernel(
     n, q,
     ids_hbm, rw_hbm, x_hbm, g_hbm, b_hbm, co_hbm, c_hbm, v_hbm, taps_hbm,
     wg_hbm, wu_hbm, wd_hbm, wo_hbm,
     gout_ref, gb_ref, gc_ref, gv_ref, ggate_ref, gup_ref, gdown_ref,
     ids_ref, rw_ref, x_ref, g_ref, b_ref, co_ref, c_ref, v_ref, taps_ref,
-    wg, wu, wd, wo, p01, p_ref, p_t, send, buf, gate, upval, dhid, hid, dg, du, turned,
+    wg, wu, wd, wo, ids_in, rw_in, x_in, g_in, p01, p_in, p_ref, p_t, send, send_in, buf, gate, upval, dhid, hid, dg, du, turned,
     part, rsib, pair, ryb, fin, ret, full_h, h_t, all_t, all_m, edge, got, padded,
-    w_sem,
+    w_sem, st, rt,
     s1, r1, sy, ry, ss, rs, s2, r2, s3, r3, s4, r4,
-    sm, rm, sp, rp, shy, rhy, shs, rhs, sa, ra, sf, rf, se, re,
+    sm, rm, shy, rhy, shs, rhs, sa, ra, sf, rf, se, re,
 ):
     s, t = lax.axis_index("sp"), lax.axis_index("tp")
     core = lax.rem(t, 2)
     sibling = t + 1 - 2 * core
-    partner = s + 1 - 2 * lax.rem(s, 2)
     ny = q // 2
     tok, cols = x_ref.shape
     total, width = part.shape
     cap = total // n
     share = width // n
     units = wg.shape[0]
-    pairs = offsets(n)
+    top = n // 2
     batch = total // 2
-    mid = n // 2
 
     barrier = pltpu.get_barrier_semaphore()
     for i in range(1, n):
@@ -86,50 +78,70 @@
     for load in [*loads[4:], *loads[:4]]:
         load.start()
 
-    def to(p):
-        k, f = pairs[p]
-        return lax.rem((partner if f else s) + 2 * k, n)
-
-    def source(p):
-        k, f = pairs[p]
-        return lax.rem((partner if f else s) - 2 * k + n, n)
-
-    def rows(p):
+    def peer(k):
+        value = s
+        for b in range(n.bit_length() - 1):
+            if k >> b & 1:
+                value = value + (1 - 2 * lax.rem(lax.div(s, 1 << b), 2)) * (1 << b)
+        return value
+
+    def rows(k):
+        p = k ^ top
         return slice(p * cap, (p + 1) * cap)
+
+    def near_rows(k):
+        return slice(k * cap, (k + 1) * cap)
 
     def at_cols(tt):
         return pl.ds(pl.multiple_of(tt * cols, cols), cols)
 
-    loads[4].wait()
-    ids0, ids1 = ids_ref[0:1, :], ids_ref[1:2, :]
-    where = lax.broadcasted_iota(jnp.int32, (n, tok), 0)
-    experts = jnp.zeros((n, tok), jnp.int32)
-    for p in range(n):
-        experts = jnp.where(where == p, to(p), experts)
-    named = jnp.logical_or(ids0 == experts, ids1 == experts)
     row_i = lax.broadcasted_iota(jnp.int32, (tok, tok), 0)
     col_i = lax.broadcasted_iota(jnp.int32, (tok, tok), 1)
-    before = jnp.dot(
-        jnp.where(named, 1.0, 0.0).astype(HALF),
-        jnp.where(row_i < col_i, 1.0, 0.0).astype(HALF),
-        preferred_element_type=F32,
-    ).astype(jnp.int32)
     slots = lax.broadcasted_iota(jnp.int32, (cap, tok), 0)
-    for p in range(n):
-        here = before[p : p + 1, :] == slots
-        c0 = jnp.where(jnp.logical_and(here, ids0 == to(p)), 1.0, 0.0)
-        c1 = jnp.where(jnp.logical_and(here, ids1 == to(p)), 1.0, 0.0)
-        p01[rows(p), 0:tok] = c0.astype(HALF)
-        p01[rows(p), tok : 2 * tok] = c1.astype(HALF)
-        p_ref[rows(p), :] = (c0 + c1).astype(HALF)
-
-    def first(a, p):
+
+    def choices(ids, ks):
+        ids0, ids1 = ids[0:1, :], ids[1:2, :]
+        where = lax.broadcasted_iota(jnp.int32, (n, tok), 0)
+        experts = jnp.full((n, tok), -1, jnp.int32)
+        for i, k in enumerate(ks):
+            experts = jnp.where(where == i, peer(k), experts)
+        named = jnp.logical_or(ids0 == experts, ids1 == experts)
+        before = jnp.dot(
+            jnp.where(named, 1.0, 0.0).astype(HALF),
+            jnp.where(row_i < col_i, 1.0, 0.0).astype(HALF),
+            preferred_element_type=F32,
+        ).astype(jnp.int32)
+        for i, k in enumerate(ks):
+            here = before[i : i + 1, :] == slots
+            c0 = jnp.where(jnp.logical_and(here, ids0 == peer(k)), 1.0, 0.0)
+            c1 = jnp.where(jnp.logical_and(here, ids1 == peer(k)), 1.0, 0.0)
+            yield k, c0, c1
+
+    def weighted(rw, g):
+        grad = g[...].astype(F32)
+        parts = []
+        for k in range(2):
+            column = jnp.sum(
+                jnp.where(row_i == col_i, rw[k : k + 1, :], 0.0), axis=1, keepdims=True
+            )
+            parts.append((column * grad).astype(HALF))
+        return jnp.concatenate(parts, axis=0)
+
+    def tokens_out(i):
+        here, there = ((ids_ref, ids_in), (x_ref, x_in), (rw_ref, rw_in), (g_ref, g_in))[i]
+        return remote(here, there, st.at[i], rt.at[i], (peer(top), t))
+
+    def first(a, k):
+        if k < top:
+            rows_out = send.at[a, near_rows(k)]
+        else:
+            rows_out = send_in.at[a, near_rows(k ^ top)]
         return remote(
-            send.at[a, rows(p)],
-            buf.at[a, rows(p), at_cols(t)],
-            s1.at[a, p],
-            r1.at[a, p],
-            (to(p), t),
+            rows_out,
+            buf.at[a, rows(k), at_cols(t)],
+            s1.at[a, k],
+            r1.at[a, k],
+            (peer(k % top), t),
         )
 
     def across(a, p, d):
@@ -142,28 +154,61 @@
         b = buf.at[a, rows(p), at_cols(lax.rem(t - 2 * d + q, q))]
         return remote(b, b, ss.at[a, p, d], rs.at[a, p, d], (s, sibling))
 
-    send_order = [*range(2, n), 1]
+    near = [*range(1, top)]
+    own_ks, rest_ks = [*range(top // 2)], [*range(top // 2, top)]
+    far_ks = [*range(top, n)]
+
+    loads[4].wait()
     loads[5].wait()
-    send[0] = jnp.dot(p_ref[...], x_ref[...], preferred_element_type=F32).astype(HALF)
     pl.semaphore_wait(barrier, n - 1 + ny)
-    for p in send_order:
-        first(0, p).start()
-    buf[0, rows(0), at_cols(t)] = send[0, rows(0), :]
+    tokens_out(0).start()
+    tokens_out(1).start()
+    for k, c0, c1 in choices(ids_ref, range(top)):
+        p01[near_rows(k), 0:tok] = c0.astype(HALF)
+        p01[near_rows(k), tok : 2 * tok] = c1.astype(HALF)
+        p_ref[rows(k), :] = (c0 + c1).astype(HALF)
+    send[0] = jnp.dot(
+        p_ref[batch:total, :], x_ref[...], preferred_element_type=F32
+    ).astype(HALF)
+    for k in near:
+        first(0, k).start()
+    buf[0, rows(0), at_cols(t)] = send[0, near_rows(0), :]
     loads[6].wait()
     loads[7].wait()
-    grad = g_ref[...].astype(F32)
-    weighted = []
-    for k in range(2):
-        column = jnp.sum(
-            jnp.where(row_i == col_i, rw_ref[k : k + 1, :], 0.0), axis=1, keepdims=True
-        )
-        weighted.append((column * grad).astype(HALF))
+    tokens_out(2).start()
+    tokens_out(3).start()
     send[1] = jnp.dot(
-        p01[...], jnp.concatenate(weighted, axis=0), preferred_element_type=F32
+        p01[...], weighted(rw_ref, g_ref), preferred_element_type=F32
     ).astype(HALF)
-    for p in send_order:
-        first(1, p).start()
-    buf[1, rows(0), at_cols(t)] = send[1, rows(0), :]
+    for k in own_ks[1:]:
+        first(1, k).start()
+    buf[1, rows(0), at_cols(t)] = send[1, near_rows(0), :]
+
+    def sort_x():
+        tokens_out(0).wait_recv()
+        tokens_out(1).wait_recv()
+        for k, c0, c1 in choices(ids_in, range(top)):
+            p01[near_rows(k), 0:tok] = c0.astype(HALF)
+            p01[near_rows(k), tok : 2 * tok] = c1.astype(HALF)
+            p_in[near_rows(k), :] = (c0 + c1).astype(HALF)
+        send_in[0] = jnp.dot(
+            p_in[...], x_in[...], preferred_element_type=F32
+        ).astype(HALF)
+        for k in near:
+            first(0, k ^ top).start()
+        buf[0, rows(top), at_cols(t)] = send_in[0, near_rows(0), :]
+
+    def sort_g():
+        tokens_out(2).wait_recv()
+        tokens_out(3).wait_recv()
+        send_in[1] = jnp.dot(
+            p01[...], weighted(rw_in, g_in), preferred_element_type=F32
+        ).astype(HALF)
+        for k in near:
+            first(1, k ^ top).start()
+        for k in rest_ks:
+            first(1, k).start()
+        buf[1, rows(top), at_cols(t)] = send_in[1, near_rows(0), :]
 
     def span(h):
         return slice(h * batch, (h + 1) * batch)
@@ -178,16 +223,18 @@
             buf[0, span(h), :], wu[...], RIGHT_T, preferred_element_type=F32
         )
 
-    def back_hidden(h):
-        dhid[span(h), :] = lax.dot_general(
-            buf[1, span(h), :], wd[...], RIGHT_T, preferred_element_type=F32
+    def back_hidden(at):
+        dhid[at, :] = lax.dot_general(
+            buf[1, at, :], wd[...], RIGHT_T, preferred_element_type=F32
         )
 
     step_rows = 32
 
-    def activation(h):
+    def activation(span_at):
         def step(r, _):
-            at = pl.ds(pl.multiple_of(h * batch + r * step_rows, step_rows), step_rows)
+            at = pl.ds(
+                pl.multiple_of(span_at.start + r * step_rows, step_rows), step_rows
+            )
             z, u, dh = gate[at, :], upval[at, :], dhid[at, :]
             sig = jax.nn.sigmoid(z)
             act = z * sig
@@ -196,32 +243,42 @@
             du[at, :] = (dh * act).astype(HALF)
             return 0
 
-        lax.fori_loop(0, batch // step_rows, step, 0)
-
-    def partial(h):
+        lax.fori_loop(0, (span_at.stop - span_at.start) // step_rows, step, 0)
+
+    def partial(at):
         def step(k, _):
             here = at_cols(k)
-            part[span(h), here] = (
+            part[at, here] = (
                 lax.dot_general(
-                    dg[span(h), :], wg[:, here], PLAIN, preferred_element_type=F32
+                    dg[at, :], wg[:, here], PLAIN, preferred_element_type=F32
                 )
                 + lax.dot_general(
-                    du[span(h), :], wu[:, here], PLAIN, preferred_element_type=F32
+                    du[at, :], wu[:, here], PLAIN, preferred_element_type=F32
                 )
             ).astype(HALF)
             return 0
 
         lax.fori_loop(0, q, step, 0)
 
-    seq = [(0, 0), (1, 0), (0, 1), (1, 1)]
-    seq += [(0, p) for p in range(2, n)] + [(1, p) for p in range(2, n)]
-
-    def last_of(a, h):
-        return max(k for k, (b, p) in enumerate(seq) if b == a and p // mid == h)
-
-    drained = set()
+    far_rows = slice(0, batch)
+    far_halves = [slice(0, batch // 2), slice(batch // 2, batch)]
+    own_rows = slice(batch, batch + batch // 2)
+    rest_rows = slice(batch + batch // 2, total)
+    seq = [(a, k) for k in own_ks for a in range(2)]
+    seq += [(0, k) for k in rest_ks + far_ks] + [(1, k) for k in far_ks + rest_ks]
+    lag = 3
+    forwarded, drained = set(), set()
+
+    def forward(upto):
+        for k in range(upto + 1):
+            if k not in forwarded:
+                forwarded.add(k)
+                for d in range(1, ny):
+                    across(*seq[k], d).wait_recv()
+                    beside(*seq[k], d).start()
 
     def drain(upto):
+        forward(upto)
         for k in range(upto + 1):
             if k not in drained:
                 drained.add(k)
@@ -231,65 +288,51 @@
     def weights(k):
         loads[k].wait()
 
+    def tokens(k):
+        p = k ^ top
+        return slice(p * tok, (p + 1) * tok)
+
+    def mixed(k):
+        low = k & -k
+        return remote(
+            all_m.at[tokens(k ^ low)], all_m.at[tokens(k)], sm.at[k], rm.at[k], (peer(low), t)
+        )
+
     def mixed_own():
         for k in range(8, 13):
             loads[k].wait()
-        all_m[0:tok, :] = (b_ref[...].astype(F32) * co_ref[...].astype(F32)).astype(HALF)
+        all_m[tokens(0), :] = (b_ref[...].astype(F32) * co_ref[...].astype(F32)).astype(HALF)
+
+    def mixed_stage(low):
+        for k in range(0, n, 2 * low):
+            if k & -k == 2 * low:
+                mixed(k).wait_recv()
+        for k in range(low, n, 2 * low):
+            mixed(k).start()
 
     def turn_slots():
+        for k, c0, c1 in choices(ids_ref, far_ks):
+            p_ref[rows(k), :] = (c0 + c1).astype(HALF)
         p_t[...] = p_ref[...].astype(F32).T.astype(HALF)
 
-    hooks = {}
+    ahead, hooks = {}, {}
 
     def hook(k, *calls):
         hooks.setdefault(min(k, len(seq) - 1), []).extend(calls)
 
-    hook(1, (None, mixed_own))
-    hook(2, (None, turn_slots))
-    x_a, x_b = last_of(0, 0), last_of(0, 1)
-    d_a, d_b = last_of(1, 0), last_of(1, 1)
-    hook(x_a + 3, (x_a, lambda: (weights(0), forward_gate(0))))
-    hook(x_a + 4, (x_a, lambda: (weights(1), forward_up(0))))
-    hook(x_b + 3, (x_b, lambda: forward_gate(1)))
-    hook(x_b + 4, (x_b, lambda: forward_up(1)))
-    hook(d_a + 3, (d_a, lambda: (weights(2), back_hidden(0))))
-    hook(d_a + 4, (d_a, lambda: activation(0)))
-
-    def forward(k):
-        for d in range(1, ny):
-            across(*seq[k], d).wait_recv()
-            beside(*seq[k], d).start()
-
-    for k, (a, p) in enumerate(seq):
-        if p:
-            first(a, p).wait_recv()
-        for d in range(1, ny):
-            across(a, p, d).start()
-        beside(a, p, 0).start()
-        if k:
-            forward(k - 1)
-        for need, call in hooks.get(k, []):
-            if need is not None:
-                drain(need)
-            call()
-
-    def mixed_far(k):
-        return remote(
-            all_m.at[0:tok],
-            all_m.at[slot_of(k, 0)],
-            sm.at[k],
-            rm.at[k],
-            (lax.rem(s + 2 * k, n), t),
-        )
-
-    def slot_of(k, f):
-        p = pairs.index((k, f))
-        return slice(p * tok, (p + 1) * tok)
-
-    def mixed_near(k):
-        return remote(
-            all_m.at[slot_of(k, 0)], all_m.at[slot_of(k, 1)], sp.at[k], rp.at[k], (partner, t)
-        )
+    at = {unit: k for k, unit in enumerate(seq)}
+    x_own, x_far = at[0, top - 1], at[0, n - 1]
+    ahead[at[0, rest_ks[-1]]] = sort_x
+    ahead[at[0, top + 1]] = sort_g
+    hook(1, mixed_own)
+    hook(3, turn_slots)
+    hook(x_own + 3, lambda: (drain(x_own), weights(0), forward_gate(1)))
+    hook(x_own + 4, lambda: (weights(1), forward_up(1)))
+    hook(x_own + 5, lambda: (weights(2), back_hidden(own_rows), activation(own_rows)))
+    hook(x_far + 3, lambda: (drain(x_far), forward_gate(0)))
+    hook(x_far + 4, lambda: forward_up(0))
+    stages = [1 << b for b in reversed(range(n.bit_length() - 1))]
+    hook(len(seq) // 2, functools.partial(mixed_stage, stages[0]))
 
     def to_side(p, d):
         theirs = lax.rem(sibling + 2 * d, q)
@@ -311,7 +354,7 @@
         )
 
     def back(p):
-        return remote(fin.at[rows(p)], ret.at[rows(p)], s4.at[p], r4.at[p], (source(p), t))
+        return remote(fin.at[rows(p)], ret.at[rows(p)], s4.at[p], r4.at[p], (peer(p), t))
 
     def mine(p, d):
         value = part[rows(p), at_cols(lax.rem(t + 2 * d, q))].astype(F32)
@@ -339,50 +382,79 @@
         else:
             ret[rows(p), :] = value.astype(HALF)
 
-    near_half, far_half = [*range(2, mid), 1, 0], [*range(mid, n)]
+    def own_batch():
+        partial(own_rows)
+        for k in reversed(own_ks):
+            side_start(k)
+
+    def own_pairs():
+        for k in reversed(own_ks):
+            pair_up(k)
+
+    def far_half(h):
+        drain(at[1, far_ks[len(far_ks) // 2 - 1 if h == 0 else -1]])
+        back_hidden(far_halves[h])
+        activation(far_halves[h])
+
+    hook(x_own + 6, own_batch)
+    hook(len(seq) - 2, own_pairs, lambda: far_half(0))
+    hook(len(seq) - 1, lambda: far_half(1))
+
+    for k, (a, p) in enumerate(seq):
+        if k in ahead:
+            ahead[k]()
+        if p % top:
+            first(a, p).wait_recv()
+        for d in range(1, ny):
+            across(a, p, d).start()
+        beside(a, p, 0).start()
+        if k >= lag:
+            forward(k - lag)
+        for call in hooks.get(k, []):
+            call()
+
     forward(len(seq) - 1)
-    shifts = [k for k, f in pairs if f == 0][1:]
-    early, late = shifts[: (len(shifts) + 1) // 3], shifts[(len(shifts) + 1) // 3 :]
-    for k in early:
-        mixed_far(k).start()
-    mixed_near(0).start()
-    partial(0)
-    for p in near_half:
-        side_start(p)
-    drain(d_b)
-    back_hidden(1)
-    for p in near_half[:-1]:
-        pair_up(p)
-    activation(1)
-    finish(near_half[0])
-    partial(1)
-    for p in far_half:
-        side_start(p)
-    if len(near_half) > 2:
-        finish(near_half[1])
-    for p in far_half + [0]:
-        pair_up(p)
-    for p in near_half[2:-1] + far_half + [0]:
-        finish(p)
-    for k in early:
-        mixed_far(k).wait_recv()
-        mixed_near(k).start()
-    for k in late:
-        mixed_far(k).start()
+    partial(far_rows)
+    for k in far_ks:
+        side_start(k)
+    mixed_stage(stages[1])
+    drain(len(seq) - 1)
+    back_hidden(rest_rows)
+    for k in far_ks:
+        pair_up(k)
+    activation(rest_rows)
+    for k in reversed(own_ks):
+        finish(k)
+    partial(rest_rows)
+    for k in rest_ks:
+        side_start(k)
+    finish(far_ks[0])
+    for k in rest_ks:
+        pair_up(k)
 
     def weight_grad(left, a, target):
-        turned[...] = left[...].astype(F32).T.astype(HALF)
-
-        def step(j, _):
-            here = at_cols(j)
+        def turn():
+            turned[...] = left[...].astype(F32).T.astype(HALF)
+
+        def piece(j):
+            here = slice(j * cols, (j + 1) * cols)
             target[:, here] = lax.dot_general(
                 turned[...], buf[a, :, here], PLAIN, preferred_element_type=F32
             ).astype(HALF)
-            return 0
-
-        lax.fori_loop(0, q, step, 0)
-
-    weight_grad(hid, 1, gdown_ref)
+
+        return [turn] + [functools.partial(piece, j) for j in range(q)]
+
+    def some(work, count):
+        for _ in range(min(count, len(work))):
+            work.pop(0)()
+
+    work = weight_grad(hid, 1, gdown_ref)
+    for i, k in enumerate(far_ks[1:] + rest_ks):
+        some(work, 1)
+        finish(k)
+        if 2 + i < len(stages):
+            mixed_stage(stages[2 + i])
+    some(work, len(work))
     for p in range(1, n):
         back(p).wait_recv()
     moe = jnp.dot(p_t[...], ret[...], preferred_element_type=F32)
@@ -405,7 +477,8 @@
 
     turn_h(t)
     weights(3)
-    weight_grad(dg, 0, ggate_ref)
+    work = weight_grad(dg, 0, ggate_ref)
+    some(work, len(work))
     h_beside(0).wait_recv()
     turn_h(sibling)
     for d in range(1, ny):
@@ -423,22 +496,20 @@
             pl.multiple_of(first_row + core * part_share, part_share), part_share
         )
 
-    def tokens(p):
-        return slice(p * tok, (p + 1) * tok)
-
     def h_far(p):
         return remote(
-            h_t.at[half_rows(to(p) * share)],
+            h_t.at[half_rows(peer(p) * share)],
             all_t.at[half_rows(0), tokens(p)],
             sa.at[p],
             ra.at[p],
-            (to(p), t),
+            (peer(p), t),
         )
 
     def h_pass(p):
         b = all_t.at[half_rows(0), tokens(p)]
         return remote(b, b, sf.at[p], rf.at[p], (s, sibling))
 
+    send_order = [*far_ks, *rest_ks, *own_ks[1:]]
     for p in send_order:
         h_far(p).start()
     all_t[:, tokens(0)] = h_t[pl.ds(pl.multiple_of(s * share, share), share), :]
@@ -455,10 +526,13 @@
     halo(1).start()
     gb_ref[...] = (grad_z * co_ref[...].astype(F32)).astype(HALF)
     padded[8 : 8 + tok, :] = dconv
-    for k in late:
-        mixed_far(k).wait_recv()
-        mixed_near(k).start()
-    weight_grad(du, 0, gup_ref)
+    work = weight_grad(du, 0, gup_ref)
+    some(work, 3)
+    for p in send_order:
+        some(work, 1)
+        h_far(p).wait_recv()
+        h_pass(p).start()
+    some(work, len(work))
     halo(0).wait_recv()
     halo(1).wait_recv()
     padded[0:8, :] = jnp.where(s > 0, got[0], 0.0)
@@ -470,18 +544,15 @@
     )
     gc_ref[...] = (grad_u * v_ref[...].astype(F32)).astype(HALF)
     gv_ref[...] = (grad_u * c_ref[...].astype(F32)).astype(HALF)
-    for p in send_order:
-        h_far(p).wait_recv()
-        h_pass(p).start()
-    for k in [0, *early, *late]:
-        mixed_near(k).wait_recv()
+    for k in range(1, n, 2):
+        mixed(k).wait_recv()
     for p in send_order:
         h_pass(p).wait_recv()
     gout_ref[...] = jnp.dot(all_t[...], all_m[...], preferred_element_type=F32)
 
     for p in range(n):
         for a in range(2):
-            if p:
+            if p % top:
                 first(a, p).wait_send()
             for d in range(1, ny):
                 across(a, p, d).wait_send()
@@ -495,14 +566,13 @@
             back(p).wait_send()
             h_far(p).wait_send()
             h_pass(p).wait_send()
+            mixed(p).wait_send()
     for d in range(ny):
         if d:
             h_across(d).wait_send()
         h_beside(d).wait_send()
-    for k in [0, *early, *late]:
-        if k:
-            mixed_far(k).wait_send()
-        mixed_near(k).wait_send()
+    for i in range(4):
+        tokens_out(i).wait_send()
     halo(0).wait_send()
     halo(1).wait_send()
 
@@ -528,7 +598,7 @@
 
     sems = [
         (2, n), (2, n, far), (2, n, ny), (n, ny), (n, far), (n,),
-        (n // 2,), (n // 2,), (far,), (ny,), (n,), (n,), (2,),
+        (n,), (far,), (ny,), (n,), (n,), (2,),
     ]
     return pl.pallas_call(
         functools.partial(layer_kernel, n, q),
@@ -551,10 +621,16 @@
             half(units, width),
             half(units, width),
             half(width, cols),
-            half(total, 2 * tok),
+            pltpu.VMEM(ids_t.shape, ids_t.dtype),
+            full(*weight_t.shape),
+            half(tok, cols),
+            half(tok, cols),
+            half(total // 2, 2 * tok),
+            half(total // 2, tok),
             half(total, tok),
             half(tok, total),
-            half(2, total, cols),
+            half(2, total // 2, cols),
+            half(2, total // 2, cols),
             half(2, total, width),
             full(total, units),
             full(total, units),
@@ -577,6 +653,8 @@
             full(2, 8, cols),
             full(tok + 16, cols),
             dma((13,)),
+            dma((4,)),
+            dma((4,)),
         ]
         + [dma(shape) for shape in sems for _ in range(2)],
         compiler_params=pltpu.CompilerParams(

time: 91.1 us -> 79.4 us (0.87)
  Pallas kernels: 90.3 us -> 78.4 us
    pallas_call x1, Pallas kernels: 86.4 us -> 74.6 us  [layer(): pl.pallas_call(functools.partial(layer_kernel, n, q), out_shape=(pltpu.VM...]
where the time goes in v2:
time: 79.4 us; the launch traced here: 79.2 us
  Pallas kernels  78.4 us (99%)
  between operations  0.81 us (1%)
    pallas_call x1, Pallas kernels, layer(): pl.pallas_call(functools.partial(layer_kernel, n, q), out_shape=(pltpu.VM...  74.6 us
    pallas_call x1, Pallas kernels, settle(): pl.pallas_call(settle_kernel, out_shape=tuple((pltpu.HBM(a.shape, a.dtype...  3.84 us

profile of v2, /device:TPU:0, one launch (start us, length us, event | category | flops | bytes accessed | tf_op | source)
XLA Modules:
  0.0 79.2 jit_solution(17553821104302348359)
XLA Ops:
  0.6 74.6 %layer.1 = (f32[256,512]{1,0:T(8,128)S(1)}, bf16[128,512]{1,0:T(8,128)(2,1)S(1)}, bf16[128,512]{1,0:T(8,128)(2,1)S(1)}, bf16[128,512]{1,0:T(8,128)(2,1)S(1)}, bf...) custom-call(s32[2,128]{1,0:T(2,128)} %bitcast.19, f32[2,128]{1,0:T(2,128)} %bitcast.20, ...), custom_call_target="tpu_custom_call" | custom-call | tf_op jit(solution)/shard_map/layer/pallas_call | solution.py:603
  75.2 3.8 %settle.1 = (f32[256,512]{1,0:T(8,128)}, bf16[128,512]{1,0:T(8,128)(2,1)}, bf16[128,512]{1,0:T(8,128)(2,1)}, bf16[128,512]{1,0:T(8,128)(2,1)}, bf16[704,2048]{1,...) custom-call(f32[256,512]{1,0:T(8,128)S(1)} %get-tuple-element.21.refs_0_, ...), custom_call_target="tpu_custom_call" | custom-call | tf_op jit(solution)/shard_map/settle/pallas_call | solution.py:685

commit v3 on v2

--- a/solution.py
+++ b/solution.py
@@ -210,18 +210,11 @@
             first(1, k).start()
         buf[1, rows(top), at_cols(t)] = send_in[1, near_rows(0), :]
 
-    def span(h):
-        return slice(h * batch, (h + 1) * batch)
-
-    def forward_gate(h):
-        gate[span(h), :] = lax.dot_general(
-            buf[0, span(h), :], wg[...], RIGHT_T, preferred_element_type=F32
-        )
-
-    def forward_up(h):
-        upval[span(h), :] = lax.dot_general(
-            buf[0, span(h), :], wu[...], RIGHT_T, preferred_element_type=F32
-        )
+    def forward_units(at):
+        for values, w in ((gate, wg), (upval, wu)):
+            values[at, :] = lax.dot_general(
+                buf[0, at, :], w[...], RIGHT_T, preferred_element_type=F32
+            )
 
     def back_hidden(at):
         dhid[at, :] = lax.dot_general(
@@ -245,27 +238,22 @@
 
         lax.fori_loop(0, (span_at.stop - span_at.start) // step_rows, step, 0)
 
-    def partial(at):
-        def step(k, _):
-            here = at_cols(k)
-            part[at, here] = (
-                lax.dot_general(
-                    dg[at, :], wg[:, here], PLAIN, preferred_element_type=F32
-                )
-                + lax.dot_general(
-                    du[at, :], wu[:, here], PLAIN, preferred_element_type=F32
-                )
-            ).astype(HALF)
-            return 0
-
-        lax.fori_loop(0, q, step, 0)
-
-    far_rows = slice(0, batch)
-    far_halves = [slice(0, batch // 2), slice(batch // 2, batch)]
-    own_rows = slice(batch, batch + batch // 2)
-    rest_rows = slice(batch + batch // 2, total)
+    def partial(at, tt):
+        here = at_cols(tt)
+        part[at, here] = (
+            lax.dot_general(dg[at, :], wg[:, here], PLAIN, preferred_element_type=F32)
+            + lax.dot_general(du[at, :], wu[:, here], PLAIN, preferred_element_type=F32)
+        ).astype(HALF)
+
+    far_rows, more_rows, own_rows, rest_rows = (
+        slice(i * batch // 2, (i + 1) * batch // 2) for i in range(4)
+    )
+    more_ks = far_ks[len(far_ks) // 2 :]
+    near_far_ks = far_ks[: len(far_ks) // 2]
+
     seq = [(a, k) for k in own_ks for a in range(2)]
-    seq += [(0, k) for k in rest_ks + far_ks] + [(1, k) for k in far_ks + rest_ks]
+    seq += [(0, k) for k in rest_ks + far_ks[:-1]] + [(1, far_ks[0]), (0, far_ks[-1])]
+    seq += [(1, k) for k in far_ks[1:] + rest_ks]
     lag = 3
     forwarded, drained = set(), set()
 
@@ -323,16 +311,20 @@
     at = {unit: k for k, unit in enumerate(seq)}
     x_own, x_far = at[0, top - 1], at[0, n - 1]
     ahead[at[0, rest_ks[-1]]] = sort_x
-    ahead[at[0, top + 1]] = sort_g
+    ahead[at[0, more_ks[0]]] = lambda: (forward(x_own), sort_g())
+    stages = [1 << b for b in reversed(range(n.bit_length() - 1))]
     hook(1, mixed_own)
     hook(3, turn_slots)
-    hook(x_own + 3, lambda: (drain(x_own), weights(0), forward_gate(1)))
-    hook(x_own + 4, lambda: (weights(1), forward_up(1)))
-    hook(x_own + 5, lambda: (weights(2), back_hidden(own_rows), activation(own_rows)))
-    hook(x_far + 3, lambda: (drain(x_far), forward_gate(0)))
-    hook(x_far + 4, lambda: forward_up(0))
-    stages = [1 << b for b in reversed(range(n.bit_length() - 1))]
-    hook(len(seq) // 2, functools.partial(mixed_stage, stages[0]))
+    hook(
+        at[1, far_ks[0]],
+        lambda: (drain(x_own), weights(0), weights(1), forward_units(slice(batch, total))),
+    )
+    hook(
+        x_far,
+        functools.partial(mixed_stage, stages[0]),
+        lambda: (drain(at[1, own_ks[-1]]), weights(2), back_hidden(own_rows)),
+        lambda: activation(own_rows),
+    )
 
     def to_side(p, d):
         theirs = lax.rem(sibling + 2 * d, q)
@@ -360,9 +352,20 @@
         value = part[rows(p), at_cols(lax.rem(t + 2 * d, q))].astype(F32)
         return value + rsib[d, rows(p), :].astype(F32)
 
-    def side_start(p):
+    def input_grads(at, ks, pairs_too, done=()):
         for d in [*range(1, ny), 0]:
-            to_side(p, d).start()
+            partial(at, lax.rem(sibling + 2 * d, q))
+            for k in ks:
+                to_side(k, d).start()
+            if pairs_too and d == 0:
+                for k in ks:
+                    pair_up(k)
+                for k in done[len(done) // 2 :]:
+                    finish(k)
+            partial(at, lax.rem(t + 2 * d, q))
+            if d == ny - 1:
+                for k in done[: len(done) // 2]:
+                    finish(k)
 
     def pair_up(p):
         for d in range(1, ny):
@@ -382,23 +385,18 @@
         else:
             ret[rows(p), :] = value.astype(HALF)
 
-    def own_batch():
-        partial(own_rows)
-        for k in reversed(own_ks):
-            side_start(k)
-
     def own_pairs():
         for k in reversed(own_ks):
             pair_up(k)
 
-    def far_half(h):
-        drain(at[1, far_ks[len(far_ks) // 2 - 1 if h == 0 else -1]])
-        back_hidden(far_halves[h])
-        activation(far_halves[h])
-
-    hook(x_own + 6, own_batch)
-    hook(len(seq) - 2, own_pairs, lambda: far_half(0))
-    hook(len(seq) - 1, lambda: far_half(1))
+    hook(at[1, far_ks[2]], lambda: input_grads(own_rows, own_ks[::-1], False))
+    hook(at[1, far_ks[-1]], own_pairs)
+    hook(
+        at[1, rest_ks[0]],
+        lambda: (drain(x_far), forward_units(slice(0, batch))),
+        lambda: (drain(at[1, near_far_ks[-1]]), back_hidden(far_rows)),
+        lambda: activation(far_rows),
+    )
 
     for k, (a, p) in enumerate(seq):
         if k in ahead:
@@ -413,24 +411,18 @@
         for call in hooks.get(k, []):
             call()
 
-    forward(len(seq) - 1)
-    partial(far_rows)
-    for k in far_ks:
-        side_start(k)
+    input_grads(far_rows, near_far_ks, True)
     mixed_stage(stages[1])
+    drain(at[1, far_ks[-1]])
+    back_hidden(more_rows)
+    activation(more_rows)
+    for k in reversed(own_ks):
+        finish(k)
+    input_grads(more_rows, more_ks, True, near_far_ks)
     drain(len(seq) - 1)
     back_hidden(rest_rows)
-    for k in far_ks:
-        pair_up(k)
     activation(rest_rows)
-    for k in reversed(own_ks):
-        finish(k)
-    partial(rest_rows)
-    for k in rest_ks:
-        side_start(k)
-    finish(far_ks[0])
-    for k in rest_ks:
-        pair_up(k)
+    input_grads(rest_rows, rest_ks, True, more_ks)
 
     def weight_grad(left, a, target):
         def turn():
@@ -449,11 +441,12 @@
             work.pop(0)()
 
     work = weight_grad(hid, 1, gdown_ref)
-    for i, k in enumerate(far_ks[1:] + rest_ks):
+    some(work, 2)
+    for low in stages[2:]:
+        mixed_stage(low)
+    for i, k in enumerate(rest_ks):
         some(work, 1)
         finish(k)
-        if 2 + i < len(stages):
-            mixed_stage(stages[2 + i])
     some(work, len(work))
     for p in range(1, n):
         back(p).wait_recv()

time: 79.4 us -> 73.2 us (0.922)
  Pallas kernels: 78.4 us -> 72.2 us
    pallas_call x1, Pallas kernels: 74.6 us -> 68.3 us  [layer(): pl.pallas_call(functools.partial(layer_kernel, n, q), out_shape=(pltpu.VM...]
where the time goes in v3:
time: 73.2 us; the launch traced here: 73 us
  Pallas kernels  72.2 us (99%)
  between operations  0.81 us (1%)
    pallas_call x1, Pallas kernels, layer(): pl.pallas_call(functools.partial(layer_kernel, n, q), out_shape=(pltpu.VM...  68.3 us
    pallas_call x1, Pallas kernels, settle(): pl.pallas_call(settle_kernel, out_shape=tuple((pltpu.HBM(a.shape, a.dtype...  3.84 us

profile of v3, /device:TPU:0, one launch (start us, length us, event | category | flops | bytes accessed | tf_op | source)
XLA Modules:
  0.0 73.0 jit_solution(2740207442604468895)
XLA Ops:
  0.6 68.3 %layer.1 = (f32[256,512]{1,0:T(8,128)S(1)}, bf16[128,512]{1,0:T(8,128)(2,1)S(1)}, bf16[128,512]{1,0:T(8,128)(2,1)S(1)}, bf16[128,512]{1,0:T(8,128)(2,1)S(1)}, bf...) custom-call(s32[2,128]{1,0:T(2,128)} %bitcast.19, f32[2,128]{1,0:T(2,128)} %bitcast.20, ...), custom_call_target="tpu_custom_call" | custom-call | tf_op jit(solution)/shard_map/layer/pallas_call | solution.py:596
  69.0 3.8 %settle.1 = (f32[256,512]{1,0:T(8,128)}, bf16[128,512]{1,0:T(8,128)(2,1)}, bf16[128,512]{1,0:T(8,128)(2,1)}, bf16[128,512]{1,0:T(8,128)(2,1)}, bf16[704,2048]{1,...) custom-call(f32[256,512]{1,0:T(8,128)S(1)} %get-tuple-element.21.refs_0_, ...), custom_call_target="tpu_custom_call" | custom-call | tf_op jit(solution)/shard_map/settle/pallas_call | solution.py:678
